TPU v7x, 256 devices: a whole 4x4x8 slice. The times are simulated.
256 devices in a mesh: fs: 32 (over z, y), tp: 8 (over x, core).
Axes of the slice: x: 4, y: 4, z: 8, core: 2. Of those that a mesh axis runs over, the one named last changes fastest.
Arguments:
- tokens: bfloat16 [32768, 2048], P(('fs', 'tp')), may hold values from -6 to 6
- norm_one: float32 [2048], replicated, may hold values from 0.1 to 1.9
- gate_one: bfloat16 [2048, 4608], P('fs', 'tp'), may hold values from -0.125 to 0.125
- up_one: bfloat16 [2048, 4608], P('fs', 'tp'), may hold values from -0.125 to 0.125
- down_one: bfloat16 [4608, 2048], P('tp', 'fs'), may hold values from -0.1875 to 0.1875
- norm_two: float32 [2048], replicated, may hold values from 0.1 to 1.9
- gate_two: bfloat16 [2048, 4608], P('fs', 'tp'), may hold values from -0.125 to 0.125
- up_two: bfloat16 [2048, 4608], P('fs', 'tp'), may hold values from -0.125 to 0.125
- down_two: bfloat16 [4608, 2048], P('tp', 'fs'), may hold values from -0.1875 to 0.1875
Outputs:
- result: bfloat16 [32768, 2048], P(('fs', 'tp'))
All inputs are finite; a program needn't handle non-finite values.
Results may differ from a plain program's by a relative error of at most 0.015.
Values may be sent and summed in bfloat16 or wider, within the bound.
A program may use at most 64 MiB of HBM per device.

v0:
```python
import jax
import jax.numpy as jnp
from jax import lax
from jax.sharding import PartitionSpec as P

eps = 1e-06


def in_one_piece(arrays, axis, dim, along):
    widths = [a.shape[along] for a in arrays]
    both = jnp.concatenate(arrays, axis=along)
    result = lax.all_gather(both, axis, axis=dim, tiled=True)
    return tuple(jnp.split(result, [sum(widths[:k]) for k in range(1, len(widths))], axis=along))


def joined_along(parts, dim):
    shape = list(parts.shape[1:])
    shape[dim] *= parts.shape[0]
    return jnp.moveaxis(parts, 0, dim).reshape(shape)


def copy_for_each(shard, axis):
    copies = jnp.broadcast_to(shard, (lax.axis_size(axis), *shard.shape))
    return lax.all_to_all(copies, axis, split_axis=0, concat_axis=0, tiled=True)


def gathered_copies(shard, axis, dim):
    return joined_along(copy_for_each(shard, axis), dim)


def in_blocks(shard, dim, size):
    shape = shard.shape
    parts = shard.reshape(*shape[:dim], size, shape[dim] // size, *shape[dim + 1 :])
    return jnp.moveaxis(parts, dim, 0)


def summed_on_arrival(shard, axis, dim):
    parts = in_blocks(shard, dim, lax.axis_size(axis))
    arrived = lax.all_to_all(parts, axis, split_axis=0, concat_axis=0, tiled=True)
    return arrived.astype(jnp.float32).sum(axis=0)


def normalize(rows, gain):
    values = rows.astype(jnp.float32)
    scaled = values * lax.rsqrt(jnp.mean(values * values, axis=-1, keepdims=True) + eps)
    return (scaled * gain).astype(jnp.bfloat16)


def hidden_units(rows, gain, gate_w, up_w):
    normed = normalize(rows, gain)
    pieces = in_one_piece((gate_w, up_w), "fs", 0, 1)
    gate_sum = jnp.dot(normed, pieces[0], preferred_element_type=jnp.float32)
    up_sum = jnp.dot(normed, pieces[1], preferred_element_type=jnp.float32)
    return (jax.nn.silu(gate_sum) * up_sum).astype(jnp.bfloat16)


def down_terms(hidden, down_w):
    return jnp.dot(hidden, gathered_copies(down_w, "fs", 1), preferred_element_type=jnp.float32)


def on_device(tokens, norm_one, gate_one, up_one, down_one, norm_two, gate_two, up_two, down_two):
    gathered = lax.all_gather(tokens, "tp", axis=0, tiled=True)
    first_terms = down_terms(hidden_units(gathered, norm_one, gate_one, up_one), down_one)
    summed = lax.psum(first_terms.astype(jnp.bfloat16), "tp").astype(jnp.float32)
    mid_group = (gathered.astype(jnp.float32) + 0.5 * summed).astype(jnp.bfloat16)
    mid_rows = lax.dynamic_slice_in_dim(
        mid_group, lax.axis_index("tp") * tokens.shape[0], tokens.shape[0], 0
    )
    second_terms = down_terms(hidden_units(mid_group, norm_two, gate_two, up_two), down_two)
    summed_two = summed_on_arrival(second_terms.astype(jnp.bfloat16), "tp", 0)
    return (mid_rows.astype(jnp.float32) + 0.5 * summed_two).astype(jnp.bfloat16)


def solution(mesh):
    return jax.shard_map(
        on_device,
        mesh=mesh,
        in_specs=(
            P(("fs", "tp"), None),
            P(),
            P("fs", "tp"),
            P("fs", "tp"),
            P("tp", "fs"),
            P(),
            P("fs", "tp"),
            P("fs", "tp"),
            P("tp", "fs"),
        ),
        out_specs=P(("fs", "tp"), None),
        check_vma=False,
    )
```

profile of v0, /device:TPU:1, one launch (start us, length us, event | category | flops | bytes accessed | tf_op | source)
XLA Modules:
  0.0 405.3 jit_solution(11405751123807447278)
XLA Ops:
  6.5 0.0 all-gather.4.cloned.1.call-start
  6.5 0.7 all-gather.4.cloned.1.call-update
  7.3 0.0 all-gather.6.cloned.1.call-start
  7.3 1.7 pad_maximum_fusion
  9.0 0.0 all-gather.6.cloned.1.call-update
  9.0 2.7 broadcast_in_dim.4
  11.7 0.0 copy-start.3
  11.7 12.2 %all-to-all-start = ((bf16[32,576,64]{1,2,0:T(8,128)(2,1)}), bf16[32,576,64]{1,2,0:T(8,128)(2,1)S(1)}, u32[]{:S(2)}, u32[]{:S(2)}) async-start(bf16[32,576,64]{1,2,0:T(8,128)(2,1)} %broadcast_in_dim.4), calls=%async_computation | async-start | bytes 5242880 | tf_op jit(solution)/shard_map/all_to_all | solution.py:24
  23.9 0.0 all-reduce.2.cloned.1.call-start
  23.9 24.0 %all-gather.4.cloned.1.call-done = bf16[1024,2048]{1,0:T(8,128)(2,1)} async-done(((bf16[128,2048]{1,0:T(8,128)(2,1)}), bf16[1024,2048]{1,0:T(8,128)(2,1)}) %all-gather.4.cloned.1.call-update) | async-done | bytes 4194320 | tf_op jit(solution)/shard_map/all_gather | solution.py:62
  48.0 3.1 fusion.3
  51.1 83.5 %all-gather.6.cloned.1.call-done = bf16[2048,1152]{1,0:T(8,128)(2,1)} async-done(((bf16[64,1152]{1,0:T(8,128)(2,1)}), bf16[2048,1152]{1,0:T(8,128)(2,1)}) %all-gather.6.cloned.1.call-update) | async-done | bytes 4718608 | tf_op jit(solution)/shard_map/all_gather | solution.py:12
  134.6 0.0 copy-done.3
  134.6 7.2 %fusion.13 = f32[1024,576]{0,1:T(8,128)} fusion(bf16[2048,1152]{1,0:T(8,128)(2,1)} %all-gather.6.cloned.1.call-done, bf16[1024,2048]{1,0:T(8,128)(2,1)} %all-gather.4.cloned.1.call-done, f32[2048]{0:T(1024)S(1)} %copy-done.3, f32[1024]{0:T(1024)S(1)} %add_rsqrt_fusion.1), kind=kOutput, calls=%fused_computation.21 | convolution fusion | flops 2424307712 | bytes 9187328 | tf_op jit(solution)/shard_map/dot_general | solution.py:52
  141.8 0.0 all-to-all-done
  141.8 13.0 %convolution_convert_fusion.1 = bf16[1024,2048]{1,0:T(8,128)(2,1)} fusion(bf16[576,2048]{0,1:T(8,128)(2,1)S(1)} %bitcast.11, f32[1024,576]{0,1:T(8,128)} %fusion.13, bf16[2048,1152]{1,0:T(8,128)(2,1)} %all-gather.6.cloned.1.call-done, bf16[1024,2048]{1,0:T(8,128)(2,1)} %all-gather.4.cloned.1.call-done, f32[2048]{0:T(1024)S(1)} %copy-done.3, ...), kind=kOutput, calls=%fused_computation.14 | convolution fusion | flops 4845862912 | bytes 15740928 | tf_op jit(solution)/shard_map/dot_general | solution.py:58
  154.8 0.0 copy-start
  154.8 0.0 copy-start.1
  154.8 0.0 copy-start.2
  154.8 0.0 all-reduce.2.cloned.1.call-update
  154.8 0.0 all-gather.8.cloned.1.call-start
  154.9 0.8 copy-done
  155.7 0.0 copy-done.1
  155.7 0.8 pad_maximum_fusion.1
  156.4 0.0 all-gather.8.cloned.1.call-update
  156.5 0.0 copy-done.2
  156.5 1.8 broadcast_in_dim.5
  158.3 5.9 %all-to-all-start.1 = ((bf16[32,576,64]{1,2,0:T(8,128)(2,1)}), bf16[32,576,64]{1,2,0:T(8,128)(2,1)S(1)}, u32[]{:S(2)}, u32[]{:S(2)}) async-start(bf16[32,576,64]{1,2,0:T(8,128)(2,1)} %broadcast_in_dim.5), calls=%async_computation.1 | async-start | bytes 5242880 | tf_op jit(solution)/shard_map/all_to_all | solution.py:24
  164.3 0.0 copy-start.4
  164.3 68.2 %all-reduce.2.cloned.1.call-done = bf16[1024,2048]{1,0:T(8,128)(2,1)} async-done(((bf16[1024,2048]{1,0:T(8,128)(2,1)}), bf16[1024,2048]{1,0:T(8,128)(2,1)}) %all-reduce.2.cloned.1.call-update) | async-done | bytes 4194320 | tf_op jit(solution)/shard_map/psum | solution.py:64
  232.5 6.0 %fusion = (f32[1024]{0:T(1024)S(1)}, bf16[1024,2048]{1,0:T(8,128)(2,1)}) fusion(bf16[1024,2048]{1,0:T(8,128)(2,1)} %all-reduce.2.cloned.1.call-done, bf16[1024,2048]{1,0:T(8,128)(2,1)} %all-gather.4.cloned.1.call-done), kind=kLoop, calls=%fused_computation.5 | loop fusion | flops 16776192 | bytes 12587008 | tf_op jit(solution)/shard_map/reduce_sum | solution.py:45
  238.4 77.5 %all-gather.8.cloned.1.call-done = bf16[2048,1152]{1,0:T(8,128)(2,1)} async-done(((bf16[64,1152]{1,0:T(8,128)(2,1)}), bf16[2048,1152]{1,0:T(8,128)(2,1)}) %all-gather.8.cloned.1.call-update) | async-done | bytes 4718608 | tf_op jit(solution)/shard_map/all_gather | solution.py:12
  315.9 0.0 copy-done.4
  315.9 7.2 %fusion.9 = f32[1024,576]{0,1:T(8,128)} fusion(bf16[2048,1152]{1,0:T(8,128)(2,1)} %all-gather.8.cloned.1.call-done, bf16[1024,2048]{1,0:T(8,128)(2,1)} %get-tuple-element.6, f32[2048]{0:T(1024)S(1)} %copy-done.4, f32[1024]{0:T(1024)S(1)} %add_rsqrt_fusion), kind=kOutput, calls=%fused_computation.17 | convolution fusion | flops 2424307712 | bytes 9187328 | tf_op jit(solution)/shard_map/dot_general | solution.py:52
  323.1 0.0 all-to-all-done.1
  323.2 13.0 %convolution_convert_fusion = bf16[1024,2048]{1,0:T(8,128)(2,1)} fusion(bf16[576,2048]{0,1:T(8,128)(2,1)S(1)} %bitcast.10, f32[1024,576]{0,1:T(8,128)} %fusion.9, bf16[2048,1152]{1,0:T(8,128)(2,1)} %all-gather.8.cloned.1.call-done, bf16[1024,2048]{1,0:T(8,128)(2,1)} %get-tuple-element.6, f32[2048]{0:T(1024)S(1)} %copy-done.4, f32[1024]{0:T(1024)S(1)} %add_rsqrt_fusion), kind=kOutput, calls=%fused_computation.13 | convolution fusion | flops 4845862912 | bytes 15740928 | tf_op jit(solution)/shard_map/dot_general | solution.py:58
  336.2 8.8 %all-to-all-start.2 = ((bf16[8,128,2048]{2,1,0:T(8,128)(2,1)}), bf16[8,128,2048]{2,1,0:T(8,128)(2,1)}, u32[]{:S(2)}, u32[]{:S(2)}) async-start(bf16[8,128,2048]{2,1,0:T(8,128)(2,1)} %bitcast.9), calls=%async_computation.2 | async-start | bytes 8388608 | tf_op jit(solution)/shard_map/all_to_all | solution.py:39
  345.0 48.8 %all-to-all-done.2 = bf16[8,128,2048]{2,1,0:T(8,128)(2,1)} async-done(((bf16[8,128,2048]{2,1,0:T(8,128)(2,1)}), bf16[8,128,2048]{2,1,0:T(8,128)(2,1)}, u32[]{:S(2)}, u32[]{:S(2)}) %all-to-all-start.2) | async-done | bytes 4194336 | tf_op jit(solution)/shard_map/all_to_all | solution.py:39
  393.8 3.0 convert_reduce_fusion
  396.8 2.0 add_convert_fusion
  (2 shorter events, 0.0 us)
Async XLA Ops:
  6.5 41.5 %all-gather.4.cloned.1.call-start = ((), (), s32[]{:S(2)}) async-start(), calls=%async_computation.3 | async-start | bytes 4718592 | tf_op jit(solution)/shard_map/all_gather | solution.py:62
  7.3 127.3 %all-gather.6.cloned.1.call-start = ((), (), s32[]{:S(2)}) async-start(), calls=%async_computation.4 | async-start | bytes 4866048 | tf_op jit(solution)/shard_map/all_gather | solution.py:12
  11.7 122.8 %copy-start.3 = (f32[2048]{0:T(1024)S(1)}, f32[2048]{0:T(1024)}, u32[]{:S(2)}) copy-start(f32[2048]{0:T(1024)} %param.10) | copy-start | bytes 24580
  11.7 130.0 %all-to-all-start = ((bf16[32,576,64]{1,2,0:T(8,128)(2,1)}), bf16[32,576,64]{1,2,0:T(8,128)(2,1)S(1)}, u32[]{:S(2)}, u32[]{:S(2)}) async-start(bf16[32,576,64]{1,2,0:T(8,128)(2,1)} %broadcast_in_dim.4), calls=%async_computation | async-start | bytes 5242880 | tf_op jit(solution)/shard_map/all_to_all | solution.py:24
  23.9 208.6 %all-reduce.2.cloned.1.call-start = ((), (), s32[]{:S(2)}) async-start(), calls=%async_computation.5 | async-start | bytes 8388608 | tf_op jit(solution)/shard_map/psum | solution.py:64
  154.8 0.9 copy-start
  154.8 0.9 copy-start.1
  154.8 1.7 copy-start.2
  154.8 161.1 %all-gather.8.cloned.1.call-start = ((), (), s32[]{:S(2)}) async-start(), calls=%async_computation.6 | async-start | bytes 4866048 | tf_op jit(solution)/shard_map/all_gather | solution.py:12
  158.3 164.8 %all-to-all-start.1 = ((bf16[32,576,64]{1,2,0:T(8,128)(2,1)}), bf16[32,576,64]{1,2,0:T(8,128)(2,1)S(1)}, u32[]{:S(2)}, u32[]{:S(2)}) async-start(bf16[32,576,64]{1,2,0:T(8,128)(2,1)} %broadcast_in_dim.5), calls=%async_computation.1 | async-start | bytes 5242880 | tf_op jit(solution)/shard_map/all_to_all | solution.py:24
  164.3 151.7 %copy-start.4 = (f32[2048]{0:T(1024)S(1)}, f32[2048]{0:T(1024)}, u32[]{:S(2)}) copy-start(f32[2048]{0:T(1024)} %param.14) | copy-start | bytes 24580
  336.2 57.6 %all-to-all-start.2 = ((bf16[8,128,2048]{2,1,0:T(8,128)(2,1)}), bf16[8,128,2048]{2,1,0:T(8,128)(2,1)}, u32[]{:S(2)}, u32[]{:S(2)}) async-start(bf16[8,128,2048]{2,1,0:T(8,128)(2,1)} %bitcast.9), calls=%async_computation.2 | async-start | bytes 8388608 | tf_op jit(solution)/shard_map/all_to_all | solution.py:39
Sparse Core Ops, SparseCore 0:
  9.2 38.7 all-gather.3
  50.6 83.9 all-gather.5
  154.9 77.4 all-reduce.1
  234.9 80.9 all-gather.7
where the time goes:
time: 406 us; the launch traced here: 405 us
  waiting for transfers between devices  303 us (75%)
  matrix products  40.4 us (10%)
  starting transfers between devices  27 us (7%)
  other arithmetic  16.4 us (4%)
  between operations  13.2 us (3%)
  local copies, waits for them, and re-layouts  5.41 us (1%)
    all_gather x2, waiting for transfers between devices, in_one_piece(): result = lax.all_gather(both, axis, axis=dim, tiled=True)  161 us
    psum x1, waiting for transfers between devices, on_device(): lax.psum(first_terms.astype(jnp.bfloat16), 'tp').astype(jnp.float32)  68.2 us
    all_to_all x1, waiting for transfers between devices, summed_on_arrival(): lax.all_to_all(parts, axis, split_axis=0, concat_axis=0, tiled=True)  48.8 us
    dot_general x2, matrix products, down_terms(): jnp.dot(hidden, gathered_copies(down_w, 'fs', 1), preferred_element_type=...  26 us
    all_gather x1, waiting for transfers between devices, on_device(): gathered = lax.all_gather(tokens, 'tp', axis=0, tiled=True)  24 us
    all_to_all x2, starting transfers between devices, copy_for_each(): return lax.all_to_all(copies, axis, split_axis=0, concat_axis=0, tiled=True)  18.1 us
    dot_general x2, matrix products, hidden_units(): gate_sum = jnp.dot(normed, pieces[0], preferred_element_type=jnp.float32)  14.5 us
    reduce_sum x2, other arithmetic, normalize(): jnp.mean(values * values, axis=-1, keepdims=True) + eps  9.03 us
  transfers between devices with their start and end apart: 7, of which 5 were waited for; matrix products, arithmetic and copies ran while one was open for 8% of the time, Pallas kernels for 0%

commit v1 on v0

v1 whole, which is shorter than its diff:
```python
import functools

import jax
import jax.numpy as jnp
from jax import lax
from jax.experimental import pallas as pl
from jax.experimental.pallas import tpu as pltpu
from jax.sharding import PartitionSpec as P

MESH = pl.DeviceIdType.MESH
EPS = 1e-06
NZ, NY, NX = 8, 4, 4
ROWS, D = 128, 2048
GU, DK, H = 1152, 640, 576
CH = 512
SEMS = 240


class Net:
    def __init__(self, send_sems, recv_sems):
        self.send_sems, self.recv_sems = send_sems, recv_sems
        self.index, self.sent = {}, []

    def slot(self, key):
        return self.index.setdefault(key, len(self.index))

    def send(self, key, src, dst, device):
        k = self.slot(key)
        copy = pltpu.make_async_remote_copy(
            src_ref=src,
            dst_ref=dst,
            send_sem=self.send_sems.at[k],
            recv_sem=self.recv_sems.at[k],
            device_id=device,
            device_id_type=MESH,
        )
        copy.start()
        self.sent.append(copy)

    def recv(self, key, ref, device):
        k = self.slot(key)
        pltpu.make_async_remote_copy(
            src_ref=ref,
            dst_ref=ref,
            send_sem=self.send_sems.at[k],
            recv_sem=self.recv_sems.at[k],
            device_id=device,
            device_id_type=MESH,
        ).wait_recv()

    def finish(self):
        for copy in self.sent:
            copy.wait_send()


def kernel(
    x_in, gu1_in, d1_in, gu2_in, d2_in, gain1, gain2, out_ref,
    xown, mid, wg1, wg2, wd1, wd2, xn1, xn2, acc, hid, keep,
    sb, rb, u1, u2, r1, r2, local_sems, send_sems, recv_sems,
):
    fs, tp = lax.axis_index("fs"), lax.axis_index("tp")
    z, y = lax.div(fs, NY), lax.rem(fs, NY)
    x, c = lax.div(tp, 2), lax.rem(tp, 2)
    oc = 1 - c

    def zz(k):
        return lax.rem(z + k + NZ, NZ)

    def yy(k):
        return lax.rem(y + k + NY, NY)

    def xx(k):
        return lax.rem(x + k + NX, NX)

    zdev = {s: (zz(s) * NY + y, tp) for s in (1, -1)}
    ydev = {s: (z * NY + yy(s), tp) for s in (1, -1)}
    xdev = {s: (fs, xx(s) * 2 + c) for s in (1, -1)}
    sib = (fs, x * 2 + oc)
    net = Net(send_sems, recv_sems)

    local = [
        pltpu.make_async_copy(src, dst, local_sems.at[k])
        for k, (src, dst) in enumerate(
            [
                (gu1_in, wg1.at[y, z]),
                (d1_in, wd1.at[z, y]),
                (x_in, xown),
                (gu2_in, wg2.at[y, z]),
                (d2_in, wd2.at[z, y]),
            ]
        )
    ]
    for copy in local:
        copy.start()

    barrier = pltpu.get_barrier_semaphore()
    for dev in (*zdev.values(), *ydev.values(), *xdev.values(), sib):
        pl.semaphore_signal(barrier, inc=1, device_id=dev, device_id_type=MESH)
    pl.semaphore_wait(barrier, 7)

    class Weights:
        def __init__(self, n, wg, wd):
            self.n, self.wg, self.wd = n, wg, wd

        def origin(self, i):
            if i == 0:
                return 0, 0, z
            s, k = (1, (i + 1) // 2) if i % 2 else (-1, i // 2)
            return s, k, zz(-s * k)

        def b1_start(self):
            for s in (1, -1):
                ref = self.wg.at[y, z]
                net.send((self.n, "b1", s, 1), ref, ref, zdev[s])

        def acquire(self, i):
            s, k, o = self.origin(i)
            ref = self.wg.at[y, o]
            net.recv((self.n, "b1", s, k), ref, zdev[-s])
            if k < (4 if s == 1 else 3):
                net.send((self.n, "b1", s, k + 1), ref, ref, zdev[s])

        def h1(self, i):
            ref = self.wg.at[y, self.origin(i)[2]]
            for s in (1, -1):
                net.send((self.n, "h1", s, i), ref, ref, ydev[s])

        def piece(self, i):
            if i:
                self.acquire(i)
            self.h1(i)

        def h2(self, i):
            o = self.origin(i)[2]
            for s in (1, -1):
                ref = self.wg.at[yy(-s), o]
                net.recv((self.n, "h1", s, i), ref, ydev[-s])
                if (i % 2 == 0) == (s == 1):
                    net.send((self.n, "h2", i), ref, ref, ydev[s])

        def h2_wait(self, i):
            ref = self.wg.at[yy(2), self.origin(i)[2]]
            net.recv((self.n, "h2", i), ref, ydev[-1 if i % 2 == 0 else 1])

        def a1_start(self):
            ref = self.wd.at[z, y]
            for s in (1, -1):
                net.send((self.n, "a1", s), ref, ref, ydev[s])

        def a1_forward(self):
            ref = self.wd.at[z, yy(-1)]
            net.recv((self.n, "a1", 1), ref, ydev[-1])
            net.send((self.n, "a1f"), ref, ref, ydev[1])
            net.recv((self.n, "a1", -1), self.wd.at[z, yy(1)], ydev[1])

        def a2_start(self):
            net.recv((self.n, "a1f"), self.wd.at[z, yy(2)], ydev[-1])
            for q in (0, 1):
                ref = self.wd.at[z, pl.ds(2 * q, 2)]
                for s in (-1, 1):
                    net.send((self.n, "a2", s, q, 1), ref, ref, zdev[s])

        def a2_hop(self, k):
            for q in (0, 1):
                for s, last in ((-1, 4), (1, 3)):
                    if k <= last:
                        ref = self.wd.at[zz(-s * k), pl.ds(2 * q, 2)]
                        net.recv((self.n, "a2", s, q, k), ref, zdev[-s])
                        if k < last:
                            net.send((self.n, "a2", s, q, k + 1), ref, ref, zdev[s])

    w1, w2 = Weights(1, wg1, wd1), Weights(2, wg2, wd2)
    offsets = (0, -1, 1, 2)

    class Gather:
        def __init__(self, n, xn):
            self.n, self.xn = n, xn

        def put(self, src, gain):
            lane = lax.broadcasted_iota(jnp.int32, (32, 128), 1)

            @pl.loop(0, ROWS // 32)
            def _(b):
                rows = pl.ds(pl.multiple_of(b * 32, 32), 32)
                v = src[rows, :].astype(jnp.float32)
                mean = jnp.mean(v * v, axis=-1, keepdims=True)
                n = v * lax.rsqrt(mean + EPS) * gain[...]
                for j in range(4):
                    for i in range(4):
                        at = 512 * i + 128 * (j // 2)
                        one, two = n[:, at : at + 128], n[:, at + 256 : at + 384]
                        if j % 2 == 0:
                            tile = jnp.where(lane < 64, one, pltpu.roll(two, 64, 1))
                        else:
                            tile = jnp.where(lane < 64, pltpu.roll(one, 64, 1), two)
                        self.xn[j, c, x, rows, 128 * i : 128 * i + 128] = tile.astype(jnp.bfloat16)

        def g0(self, s):
            j = yy(offsets[s])
            ref = self.xn.at[j, c, x]
            for d in (1, -1):
                net.send((self.n, "g1", d, s), ref, ref, xdev[d])
            net.send((self.n, "gs", 0, s), ref, ref, sib)

        def g1(self, s):
            j = yy(offsets[s])
            for d in (1, -1):
                ref = self.xn.at[j, c, xx(-d)]
                net.recv((self.n, "g1", d, s), ref, xdev[-d])
                half = self.xn.at[j, c, xx(-d), pl.ds(0 if d == 1 else 64, 64)]
                net.send((self.n, "g2", d, s), half, half, xdev[d])
                net.send((self.n, "gs", d, s), ref, ref, sib)

        def g2(self, s):
            j = yy(offsets[s])
            for d in (1, -1):
                half = self.xn.at[j, c, xx(2), pl.ds(0 if d == 1 else 64, 64)]
                net.recv((self.n, "g2", d, s), half, xdev[-d])
            ref = self.xn.at[j, c, xx(2)]
            net.send((self.n, "gs", 2, s), ref, ref, sib)

        def g3(self, s):
            j = yy(offsets[s])
            for d, k in ((0, 0), (1, -1), (-1, 1), (2, 2)):
                net.recv((self.n, "gs", d, s), self.xn.at[j, oc, xx(k)], sib)

    def gate_up(xn, wg, s):
        j = yy(offsets[s])

        @pl.loop(0, 2)
        def _(i):
            rows = xn[j, i].reshape(4 * ROWS, CH)
            part = jnp.dot(rows, wg[j].reshape(CH, GU), preferred_element_type=jnp.float32)
            if s:
                acc[i] += part
            else:
                acc[i] = part

    def activate():
        lane = lax.broadcasted_iota(jnp.int32, (64, 128), 1)

        @pl.loop(0, 16)
        def _(b):
            i, rows = lax.div(b, 8), pl.ds(pl.multiple_of(lax.rem(b, 8) * 64, 64), 64)
            for n in range(4):
                g = acc[i, rows, 128 * n : 128 * n + 128]
                u = acc[i, rows, 512 + 128 * n : 640 + 128 * n]
                h = g / (1.0 + jnp.exp(-g)) * u
                hid[i, rows, 128 * n : 128 * n + 128] = h.astype(jnp.bfloat16)
            t = acc[i, rows, 1024:1152]
            h = t / (1.0 + jnp.exp(-t)) * pltpu.roll(t, 64, 1)
            hid[i, rows, 512:640] = jnp.where(lane < 64, h, 0.0).astype(jnp.bfloat16)

    class Scatter:
        def __init__(self, n, wd, finish):
            self.n, self.wd, self.finish = n, wd, finish

        def product(self, which, j):
            w = self.wd[2 * j : 2 * j + 2].reshape(CH, DK)
            return lax.dot_general(
                hid[which], w, (((1,), (1,)), ((), ())), preferred_element_type=jnp.float32
            )

        def s0(self, j):
            h = self.n - 1
            sb[h, j] = self.product(oc, j).astype(jnp.bfloat16).reshape(4, ROWS, CH)
            net.send((self.n, "r0", j), sb.at[h, j], rb.at[h, j], sib)
            keep[j] = self.product(c, j).reshape(4, ROWS, CH)

        def chip(self, j, k):
            h = self.n - 1
            return keep[j, xx(k)] + rb[h, j, xx(k)].astype(jnp.float32)

        def s1(self, j):
            h = self.n - 1
            net.recv((self.n, "r0", j), rb.at[h, j], sib)
            u1[h, j] = self.chip(j, 2).astype(jnp.bfloat16)
            for d in (1, -1):
                at = 0 if d == 1 else 64
                net.send(
                    (self.n, "r1", d, j), u1.at[h, j, pl.ds(at, 64)], r1.at[h, j, pl.ds(at, 64)], xdev[d]
                )

        def s2(self, j):
            h = self.n - 1
            for d in (1, -1):
                at, other = (0, 64) if d == 1 else (64, 0)
                part = r1.at[h, j, pl.ds(at, 64)]
                net.recv((self.n, "r1", d, j), part, xdev[-d])
                near = self.chip(j, d)
                both = near[at : at + 64] + part[...].astype(jnp.float32)
                e = 0 if d == 1 else 1
                u2[h, j, e, at : at + 64] = both.astype(jnp.bfloat16)
                u2[h, j, e, other : other + 64] = near[other : other + 64].astype(jnp.bfloat16)
                net.send((self.n, "r2", d, j), u2.at[h, j, e], r2.at[h, j, e], xdev[d])

        def s3(self, j):
            h = self.n - 1
            for d in (1, -1):
                net.recv((self.n, "r2", d, j), r2.at[h, j, 0 if d == 1 else 1], xdev[-d])
            total = self.chip(j, 0) + r2[h, j, 0].astype(jnp.float32) + r2[h, j, 1].astype(jnp.float32)
            self.finish(j, total)

    def cols(j):
        return slice(CH * j, CH * j + CH)

    def to_middle(j, total):
        mid[:, cols(j)] = (xown[:, cols(j)].astype(jnp.float32) + 0.5 * total).astype(jnp.bfloat16)

    def to_result(j, total):
        out_ref[:, cols(j)] = (mid[:, cols(j)].astype(jnp.float32) + 0.5 * total).astype(jnp.bfloat16)

    ga, gb = Gather(1, xn1), Gather(2, xn2)
    ra, rbk = Scatter(1, wd1, to_middle), Scatter(2, wd2, to_result)

    local[0].wait()
    w1.b1_start()
    local[1].wait()
    w1.a1_start()
    w1.h1(0)
    local[2].wait()
    ga.put(xown, gain1)
    for s in range(4):
        ga.g0(s)
    w1.piece(1)
    w1.piece(2)
    w1.a1_forward()
    w1.h2(0)
    ga.g1(0)
    w1.a2_start()
    w1.piece(3)
    w1.piece(4)
    ga.g1(1)
    w1.h2(1)
    w1.h2(2)
    w1.a2_hop(1)
    ga.g1(2)
    ga.g2(0)
    w1.piece(5)
    w1.piece(6)
    ga.g1(3)
    ga.g2(1)
    w1.h2(3)
    w1.h2(4)
    w1.a2_hop(2)
    w1.piece(7)
    ga.g2(2)
    ga.g2(3)
    local[3].wait()
    local[4].wait()
    w2.b1_start()
    w2.a1_start()
    for s in range(4):
        ga.g3(s)
    w1.h2(5)
    w1.h2(6)
    gate_up(xn1, wg1, 0)
    w1.a2_hop(3)
    w1.h2(7)
    gate_up(xn1, wg1, 1)
    w2.a1_forward()
    w2.h1(0)
    w2.piece(1)
    w2.piece(2)
    gate_up(xn1, wg1, 2)
    for i in range(8):
        w1.h2_wait(i)
    gate_up(xn1, wg1, 3)
    w1.a2_hop(4)
    w2.a2_start()
    activate()

    steps = [
        lambda: (w2.piece(3), w2.piece(4)),
        lambda: (w2.h2(0), w2.a2_hop(1)),
        lambda: (w2.piece(5), w2.piece(6)),
        lambda: (w2.h2(1), w2.h2(2)),
        lambda: (w2.piece(7), w2.a2_hop(2)),
        lambda: (w2.h2(3), w2.h2(4)),
        lambda: w2.a2_hop(3),
        lambda: (w2.h2(5), w2.h2(6)),
        lambda: w2.a2_hop(4),
        lambda: w2.h2(7),
    ]
    for t in range(7):
        for stage, do in ((3, ra.s3), (2, ra.s2), (1, ra.s1), (0, ra.s0)):
            if 0 <= t - stage < 4:
                do(t - stage)
        if steps:
            steps.pop(0)()

    gb.put(mid, gain2)
    for s in range(4):
        gb.g0(s)
    for t in range(6):
        if t < 4:
            gb.g1(t)
        if steps:
            steps.pop(0)()
        if 0 <= t - 1 < 4:
            gb.g2(t - 1)
        if 0 <= t - 2 < 4:
            gb.g3(t - 2)
            if t - 2 == 3:
                for i in range(8):
                    w2.h2_wait(i)
            gate_up(xn2, wg2, t - 2)
    activate()
    for t in range(7):
        for stage, do in ((3, rbk.s3), (2, rbk.s2), (1, rbk.s1), (0, rbk.s0)):
            if 0 <= t - stage < 4:
                do(t - stage)
    net.finish()


def layer(x, gu1, d1, gu2, d2, gain1, gain2):
    bf, f32 = jnp.bfloat16, jnp.float32
    hbm = pl.BlockSpec(memory_space=pl.ANY)
    vmem = pl.BlockSpec(memory_space=pltpu.VMEM)
    return pl.pallas_call(
        kernel,
        out_shape=jax.ShapeDtypeStruct((ROWS, D), bf),
        in_specs=[hbm] * 5 + [vmem] * 2,
        out_specs=vmem,
        scratch_shapes=[
            pltpu.VMEM((ROWS, D), bf),
            pltpu.VMEM((ROWS, D), bf),
            pltpu.VMEM((NY, NZ, 64, GU), bf),
            pltpu.VMEM((NY, NZ, 64, GU), bf),
            pltpu.VMEM((NZ, NY, 64, DK), bf),
            pltpu.VMEM((NZ, NY, 64, DK), bf),
            pltpu.VMEM((4, 2, NX, ROWS, CH), bf),
            pltpu.VMEM((4, 2, NX, ROWS, CH), bf),
            pltpu.VMEM((2, 4 * ROWS, GU), f32),
            pltpu.VMEM((2, 4 * ROWS, DK), bf),
            pltpu.VMEM((4, NX, ROWS, CH), f32),
            pltpu.VMEM((2, 4, NX, ROWS, CH), bf),
            pltpu.VMEM((2, 4, NX, ROWS, CH), bf),
            pltpu.VMEM((2, 4, ROWS, CH), bf),
            pltpu.VMEM((2, 4, 2, ROWS, CH), bf),
            pltpu.VMEM((2, 4, ROWS, CH), bf),
            pltpu.VMEM((2, 4, 2, ROWS, CH), bf),
            pltpu.SemaphoreType.DMA((5,)),
            pltpu.SemaphoreType.DMA((SEMS,)),
            pltpu.SemaphoreType.DMA((SEMS,)),
        ],
        compiler_params=pltpu.CompilerParams(
            collective_id=0, has_side_effects=True, vmem_limit_bytes=60 * 2**20
        ),
    )(x, gu1, d1, gu2, d2, gain1, gain2)


def joined(gate, up):
    return jnp.concatenate([gate[:, :512], up[:, :512], gate[:, 512:], up[:, 512:]], axis=1)


def turned(down):
    return jnp.pad(down.T, ((0, 0), (0, DK - H)))


def on_device(tokens, norm_one, gate_one, up_one, down_one, norm_two, gate_two, up_two, down_two):
    return layer(
        tokens,
        joined(gate_one, up_one),
        turned(down_one),
        joined(gate_two, up_two),
        turned(down_two),
        norm_one.reshape(1, D),
        norm_two.reshape(1, D),
    )


def solution(mesh):
    return jax.shard_map(
        on_device,
        mesh=mesh,
        in_specs=(
            P(("fs", "tp"), None),
            P(),
            P("fs", "tp"),
            P("fs", "tp"),
            P("tp", "fs"),
            P(),
            P("fs", "tp"),
            P("fs", "tp"),
            P("tp", "fs"),
        ),
        out_specs=P(("fs", "tp"), None),
        check_vma=False,
    )
```

time: 406 us -> 160 us (0.39)
  waiting for transfers between devices: 303 us -> 0 us
  Pallas kernels: 0 us -> 151 us
  matrix products: 40.4 us -> 0 us
  starting transfers between devices: 27 us -> 0 us
  other arithmetic: 16.4 us -> 0 us
  between operations: 13.2 us -> 0.03 us
    all_gather x3 -> x0, waiting for transfers between devices: 185 us -> none  [the longest x2 161 us: in_one_piece(): result = lax.all_gather(both, axis, axis=dim, tiled=True)]
    pallas_call x0 -> x1, Pallas kernels: none -> 151 us  [layer(): pl.pallas_call(kernel, out_shape=jax.ShapeDtypeStruct((ROWS, D), bf), in_...]
    psum x1 -> x0, waiting for transfers between devices: 68.2 us -> none  [on_device(): lax.psum(first_terms.astype(jnp.bfloat16), 'tp').astype(jnp.float32)]
    all_to_all x3 -> x0, waiting for transfers between devices: 48.8 us -> none  [the longest x1 48.8 us: summed_on_arrival(): lax.all_to_all(parts, axis, split_axis=0, concat_axis=0, tiled=True)]
    dot_general x4 -> x0, matrix products: 40.4 us -> none  [the longest x2 26 us: down_terms(): jnp.dot(hidden, gathered_copies(down_w, 'fs', 1), preferred_element_type=...]
    all_to_all x3 -> x0, starting transfers between devices: 26.9 us -> none  [the longest x2 18.1 us: copy_for_each(): return lax.all_to_all(copies, axis, split_axis=0, concat_axis=0, tiled=True)]
    reduce_sum x3 -> x0, other arithmetic: 12 us -> none  [the longest x2 9.03 us: normalize(): jnp.mean(values * values, axis=-1, keepdims=True) + eps]
    broadcast_in_dim x2 -> x0, local copies, waits for them, and re-layouts: 4.55 us -> none  [copy_for_each(): copies = jnp.broadcast_to(shard, (lax.axis_size(axis), *shard.shape))]
  transfers between devices with their start and end apart: 7 -> 0, of which waited for: 5 -> 0; matrix products, arithmetic and copies ran while one was open for 8% -> 0% of each run, Pallas kernels for 0% -> 0%
where the time goes in v1:
time: 160 us; the launch traced here: 158 us
  Pallas kernels  151 us (94%)
  local copies, waits for them, and re-layouts  6.84 us (4%)
    pallas_call x1, Pallas kernels, layer(): pl.pallas_call(kernel, out_shape=jax.ShapeDtypeStruct((ROWS, D), bf), in_...  151 us

profile of v1, /device:TPU:1, one launch (start us, length us, event | category | flops | bytes accessed | tf_op | source)
XLA Modules:
  0.0 158.3 jit_solution(11217237357508660801)
XLA Ops:
  0.0 0.0 slice-start.3
  0.0 0.0 slice-start
  0.0 0.0 slice-start.1
  0.0 0.0 slice-start.2
  0.0 0.8 slice-done.3
  0.8 0.0 slice-done
  0.8 0.0 slice-done.1
  0.9 0.0 slice-done.2
  0.9 0.7 concatenate.6.gu1_in
  1.6 0.0 slice-start.7
  1.6 0.0 slice-start.4
  1.6 0.0 slice-start.5
  1.6 0.0 slice-start.6
  1.7 0.8 slice-done.7
  2.5 0.0 slice-done.4
  2.5 0.0 slice-done.5
  2.5 0.0 slice-done.6
  2.5 0.0 copy-start
  2.5 0.7 concatenate.7.gu2_in
  3.3 0.1 copy-done
  3.4 0.0 copy-start.1
  3.4 0.7 pad.7.d1_in
  4.1 0.2 copy-done.1
  4.3 0.7 pad.8.d2_in
  5.0 151.4 %shard_map.91 = bf16[128,2048]{1,0:T(8,128)(2,1)} custom-call(bf16[128,2048]{1,0:T(8,128)(2,1)} %x_in.1, bf16[64,1152]{1,0:T(8,128)(2,1)} %concatenate.6.gu1_in, bf16[64,640]{1,0:T(8,128)(2,1)} %pad.7.d1_in, bf16[64,1152]{1,0:T(8,128)(2,1)} %concatenate.7.gu2_in, bf16[64,640]{1,0:T(8,128)(2,1)} %pad.8.d2_in, f32[1,2048]{1,0:T(1,128)} %bitcast.6, ...), custom_call_target="tpu_custom_call" | custom-call | tf_op jit(solution)/shard_map/pallas_call | solution.py:420
  156.4 1.9 %copy.11 = bf16[128,2048]{1,0:T(8,128)(2,1)} copy(bf16[128,2048]{1,0:T(8,128)(2,1)} %shard_map.91) | data formatting | bytes 1048576
Async XLA Ops:
  0.0 0.8 slice-start.3
  0.0 0.8 slice-start
  0.0 0.9 slice-start.1
  0.0 0.9 slice-start.2
  1.6 0.8 slice-start.7
  1.6 0.8 slice-start.4
  1.6 0.9 slice-start.5
  1.6 0.9 slice-start.6
  2.5 0.9 copy-start
  3.4 0.9 copy-start.1

commit v2 on v0

v2 whole, which is shorter than its diff:
```python
import math

import jax
import jax.numpy as jnp
from jax import lax
from jax.experimental import pallas as pl
from jax.experimental.pallas import tpu as pltpu
from jax.sharding import PartitionSpec as P

MESH = pl.DeviceIdType.MESH
EPS = 1e-06
NZ, NY, NX = 8, 4, 4
ROWS, D = 128, 2048
GA, GB = 512, 640
DA, DB = 256, 384
DK, H = DA + DB, 576
CH = 512
SEMS = 320

PER_BYTE = 1 / 46.6e3
PER_BYTE_CHIP = 1 / 500e3
HOP, HOP_CHIP = 1.9, 1.1
BACKLOG = 1.5


class Plan:
    def __init__(self):
        self.tasks = {}

    def add(self, name, rank, recv=(), work=None, time=0.0, send=(), after=()):
        self.tasks[name] = (rank, recv, work, time, send, after)

    def order(self):
        now, free, done, arrive, left, result = 0.0, {}, set(), {}, dict(self.tasks), []
        while left:
            pick, later = None, []
            for name, (rank, recv, work, time, send, after) in left.items():
                if not all(a in done for a in after) or not all(r[0] in arrive for r in recv):
                    continue
                at = max([arrive[r[0]] for r in recv], default=0.0)
                at = max([at] + [free.get(s[4], 0.0) - BACKLOG for s in send])
                if at > now:
                    later.append(at)
                elif pick is None or (rank, len(result)) < pick[:2]:
                    pick = (rank, len(result), name)
            if pick is None:
                now = min(later)
                continue
            name = pick[2]
            rank, recv, work, time, send, after = left.pop(name)
            now += time + 0.02
            for key, src, dst, device, link in send:
                size = 2 * math.prod(src.shape)
                start = max(free.get(link, 0.0), now)
                free[link] = start + size * (PER_BYTE_CHIP if link == "c" else PER_BYTE)
                arrive[key] = free[link] + (HOP_CHIP if link == "c" else HOP)
            done.add(name)
            result.append(name)
        self.model_time = now
        return result


class Net:
    def __init__(self, send_sems, recv_sems):
        self.send_sems, self.recv_sems = send_sems, recv_sems
        self.index, self.sent = {}, []

    def copy(self, key, src, dst, device):
        k = self.index.setdefault(key, len(self.index))
        return pltpu.make_async_remote_copy(
            src_ref=src,
            dst_ref=dst,
            send_sem=self.send_sems.at[k],
            recv_sem=self.recv_sems.at[k],
            device_id=device,
            device_id_type=MESH,
        )

    def send(self, key, src, dst, device):
        copy = self.copy(key, src, dst, device)
        copy.start()
        self.sent.append(copy)

    def recv(self, key, ref, device):
        self.copy(key, ref, ref, device).wait_recv()

    def finish(self):
        for copy in self.sent:
            copy.wait_send()


def kernel(
    x_in, gate1_in, up1_in, down1_in, gate2_in, up2_in, down2_in, rest_in, gain1, gain2, out_ref,
    xown, mid, ga1, gb1, ga2, gb2, da1, db1, da2, db2, xn1, xn2, acca, accb, hid, keep,
    sb, rb, u1, u2, r1, r2, local_sems, send_sems, recv_sems,
):
    fs, tp = lax.axis_index("fs"), lax.axis_index("tp")
    z, y = lax.div(fs, NY), lax.rem(fs, NY)
    x, c = lax.div(tp, 2), lax.rem(tp, 2)
    oc = 1 - c

    zs = {k: lax.rem(z + k + NZ, NZ) for k in range(-4, 5)}
    ys = {k: lax.rem(y + k + NY, NY) for k in range(-1, 3)}
    xs = {k: lax.rem(x + k + NX, NX) for k in range(-1, 3)}
    zdev = {s: (zs[s] * NY + y, tp) for s in (1, -1)}
    ydev = {s: (z * NY + ys[s], tp) for s in (1, -1)}
    xdev = {s: (fs, xs[s] * 2 + c) for s in (1, -1)}
    sib = (fs, x * 2 + oc)
    net, plan = Net(send_sems, recv_sems), Plan()

    def fetch(k, src, dst):
        copy = pltpu.make_async_copy(src, dst, local_sems.at[k])
        copy.start()
        return copy

    def lanes(ref, at, size):
        return ref.at[:, pl.ds(at, size)]

    local = {
        1: [
            fetch(0, lanes(gate1_in, 0, 512), ga1.at[y, z]),
            fetch(1, lanes(up1_in, 0, 512), lanes(gb1.at[y, z], 0, 512)),
            fetch(2, lanes(rest_in, 0, 128), lanes(gb1.at[y, z], 512, 128)),
        ],
        0: [fetch(3, x_in, xown)],
        2: [fetch(4, lanes(down1_in, 0, DA), da1.at[z, y]), fetch(5, lanes(rest_in, 128, DB), db1.at[z, y])],
        3: [
            fetch(6, lanes(gate2_in, 0, 512), ga2.at[y, z]),
            fetch(7, lanes(up2_in, 0, 512), lanes(gb2.at[y, z], 0, 512)),
            fetch(8, lanes(rest_in, 512, 128), lanes(gb2.at[y, z], 512, 128)),
        ],
        4: [fetch(9, lanes(down2_in, 0, DA), da2.at[z, y]), fetch(10, lanes(rest_in, 640, DB), db2.at[z, y])],
    }

    barrier = pltpu.get_barrier_semaphore()
    for dev in (*zdev.values(), *ydev.values(), *xdev.values(), sib):
        pl.semaphore_signal(barrier, inc=1, device_id=dev, device_id_type=MESH)
    pl.semaphore_wait(barrier, 7)

    def origin(i):
        return (1, (i + 1) // 2) if i % 2 else (-1, i // 2)

    def weights(m, part_a, pair_a, part_b):
        def land():
            for copy in local[m]:
                copy.wait()

        own_a, own_b = part_a(y, z), part_b(y, z)
        plan.add((m, "land"), m, work=land)
        plan.add(
            (m, "b1s"), m, after=[(m, "land")],
            send=[((m, "b1", s, 1), own_b, own_b, zdev[s], f"z{s}") for s in (1, -1)],
        )
        plan.add(
            (m, "a1s"), m, after=[(m, "land")],
            send=[((m, "a1", s), own_a, own_a, ydev[s], f"y{s}") for s in (1, -1)],
        )
        plan.add(
            (m, "h1", 0), m + 0.1, after=[(m, "land")],
            send=[((m, "h1", s, 0), own_b, own_b, ydev[s], f"y{s}") for s in (1, -1)],
        )
        for i in range(1, 8):
            s, k = origin(i)
            ref = part_b(y, zs[-s * k])
            more = k < (4 if s == 1 else 3)
            plan.add(
                (m, "b1", i), m, recv=[((m, "b1", s, k), ref, zdev[-s])],
                send=[((m, "b1", s, k + 1), ref, ref, zdev[s], f"z{s}")] if more else [],
            )
            plan.add(
                (m, "h1", i), m + 0.1, after=[(m, "b1", i)],
                send=[((m, "h1", e, i), ref, ref, ydev[e], f"y{e}") for e in (1, -1)],
            )
        for i in range(8):
            s, k = origin(i)
            o = zs[-s * k]
            for e in (1, -1):
                ref = part_b(ys[-e], o)
                forward = (i % 2 == 0) == (e == 1)
                plan.add(
                    (m, "h2", e, i), m, recv=[((m, "h1", e, i), ref, ydev[-e])],
                    send=[((m, "h2", i), ref, ref, ydev[e], f"y{e}")] if forward else [],
                )
            plan.add(
                (m, "h2w", i), m + 0.3,
                recv=[((m, "h2", i), part_b(ys[2], o), ydev[-1 if i % 2 == 0 else 1])],
            )
        ref = part_a(ys[-1], z)
        plan.add(
            (m, "a1", 1), m, recv=[((m, "a1", 1), ref, ydev[-1])],
            send=[((m, "a1f"), ref, ref, ydev[1], "y1")],
        )
        plan.add((m, "a1", -1), m, recv=[((m, "a1", -1), part_a(ys[1], z), ydev[1])])
        plan.add((m, "a1", 2), m, recv=[((m, "a1f"), part_a(ys[2], z), ydev[-1])])
        for q in (0, 1):
            for s, last in ((-1, 4), (1, 3)):
                ref = pair_a(q, z)
                plan.add(
                    (m, "a2", s, q, 0), m + 0.05, after=[(m, "land")] + [(m, "a1", k) for k in (1, -1, 2)],
                    send=[((m, "a2", s, q, 1), ref, ref, zdev[s], f"z{s}")],
                )
                for k in range(1, last + 1):
                    ref = pair_a(q, zs[-s * k])
                    plan.add(
                        (m, "a2", s, q, k), m + 0.05, recv=[((m, "a2", s, q, k), ref, zdev[-s])],
                        send=[((m, "a2", s, q, k + 1), ref, ref, zdev[s], f"z{s}")] if k < last else [],
                    )

    def gate_parts(a, b):
        return (
            lambda yi, zi: a.at[yi, zi],
            lambda q, zi: a.at[pl.ds(2 * q, 2), zi],
            lambda yi, zi: b.at[yi, zi],
        )

    def down_parts(a, b):
        return (
            lambda yi, zi: a.at[zi, yi],
            lambda q, zi: a.at[zi, pl.ds(2 * q, 2)],
            lambda yi, zi: b.at[zi, yi],
        )

    weights(1, *gate_parts(ga1, gb1))
    weights(2, *down_parts(da1, db1))
    weights(3, *gate_parts(ga2, gb2))
    weights(4, *down_parts(da2, db2))

    offsets = (0, -1, 1, 2)

    def gather(n, src, gain, xn, after):
        def norm():
            if n == 1:
                local[0][0].wait()
            lane = lax.broadcasted_iota(jnp.int32, (32, 128), 1)

            @pl.loop(0, ROWS // 32)
            def _(b):
                rows = pl.ds(pl.multiple_of(b * 32, 32), 32)
                v = src[rows, :].astype(jnp.float32)
                mean = jnp.mean(v * v, axis=-1, keepdims=True)
                scaled = v * lax.rsqrt(mean + EPS) * gain[...]
                for j in range(4):
                    for i in range(4):
                        at = 512 * i + 128 * (j // 2)
                        one, two = scaled[:, at : at + 128], scaled[:, at + 256 : at + 384]
                        if j % 2 == 0:
                            tile = jnp.where(lane < 64, one, pltpu.roll(two, 64, 1))
                        else:
                            tile = jnp.where(lane < 64, pltpu.roll(one, 64, 1), two)
                        xn[j, c, x, rows, 128 * i : 128 * i + 128] = tile.astype(jnp.bfloat16)

        plan.add((n, "norm"), 0.5, work=norm, time=0.9, after=after)
        for s in range(4):
            j = ys[offsets[s]]
            own = xn.at[j, c, x]
            plan.add(
                (n, "g0", s), 0.1 * s, after=[(n, "norm")],
                send=[((n, "g1", d, s), own, own, xdev[d], f"x{d}") for d in (1, -1)]
                + [((n, "gs", 0, s), own, own, sib, "c")],
            )
            halves = []
            for d in (1, -1):
                ref = xn.at[j, c, xs[-d]]
                half = xn.at[j, c, xs[-d], pl.ds(0 if d == 1 else 64, 64)]
                plan.add(
                    (n, "g1", d, s), 0.1 * s, recv=[((n, "g1", d, s), ref, xdev[-d])],
                    send=[((n, "g2", d, s), half, half, xdev[d], f"x{d}"), ((n, "gs", d, s), ref, ref, sib, "c")],
                )
                halves.append(
                    ((n, "g2", d, s), xn.at[j, c, xs[2], pl.ds(0 if d == 1 else 64, 64)], xdev[-d])
                )
            ref = xn.at[j, c, xs[2]]
            plan.add((n, "g2", s), 0.1 * s, recv=halves, send=[((n, "gs", 2, s), ref, ref, sib, "c")])
            plan.add(
                (n, "g3", s), 0.5,
                recv=[
                    ((n, "gs", d, s), xn.at[j, oc, xs[k]], sib)
                    for d, k in ((0, 0), (1, -1), (-1, 1), (2, 2))
                ],
            )

    def hidden(n, m, xn, ga, gb, after):
        started = set()

        def dot(acc, w, s):
            j = ys[offsets[s]]
            first = acc not in started
            started.add(acc)
            target = acca if acc == "a" else accb

            @pl.loop(0, 2)
            def _(i):
                rows = xn[j, i].reshape(4 * ROWS, CH)
                part = jnp.dot(rows, w[j].reshape(CH, w.shape[-1]), preferred_element_type=jnp.float32)
                if first:
                    target[i] = part
                else:
                    target[i] += part

        parts = {
            0: [(m, "land")] + [(m, "b1", i) for i in range(1, 8)],
            1: [(m, "h2", 1, i) for i in range(8)],
            2: [(m, "h2", -1, i) for i in range(8)],
            3: [(m, "h2w", i) for i in range(8)],
        }
        blocks = [(m, "a2", s, q, k) for q in (0, 1) for s, last in ((-1, 4), (1, 3)) for k in range(last + 1)]
        for s in range(4):
            plan.add(
                (n, "gub", s), 5, work=lambda s=s: dot("b", gb, s), time=0.98,
                after=[(n, "norm"), (n, "g2", s), (n, "g3", s)] + parts[s] + after,
            )
            plan.add(
                (n, "gua", s), 5, work=lambda s=s: dot("a", ga, s), time=0.8,
                after=[(n, "norm"), (n, "g2", s), (n, "g3", s)] + blocks + after,
            )

        def activate():
            lane = lax.broadcasted_iota(jnp.int32, (64, 128), 1)

            @pl.loop(0, 16)
            def _(b):
                i, rows = lax.div(b, 8), pl.ds(pl.multiple_of(lax.rem(b, 8) * 64, 64), 64)
                for k in range(4):
                    g = acca[i, rows, 128 * k : 128 * k + 128]
                    u = accb[i, rows, 128 * k : 128 * k + 128]
                    h = g / (1.0 + jnp.exp(-g)) * u
                    hid[i, rows, 128 * k : 128 * k + 128] = h.astype(jnp.bfloat16)
                t = accb[i, rows, 512:640]
                h = t / (1.0 + jnp.exp(-t)) * pltpu.roll(t, 64, 1)
                hid[i, rows, 512:640] = jnp.where(lane < 64, h, 0.0).astype(jnp.bfloat16)

        plan.add(
            (n, "act"), 5, work=activate, time=1.25,
            after=[(n, k, s) for k in ("gua", "gub") for s in range(4)],
        )

    def scatter(n, m, da, db, add):
        h = n - 1

        def product(which, i):
            s, k = origin(i)
            o = zs[-s * k]
            dims = (((1,), (1,)), ((), ()))
            return lax.dot_general(
                hid[which, :, 0:DA], da[o].reshape(256, DA), dims, preferred_element_type=jnp.float32
            ) + lax.dot_general(
                hid[which, :, DA:DK], db[o].reshape(256, DB), dims, preferred_element_type=jnp.float32
            )

        def give(j):
            for b in (0, 1):
                sb[h, j, b] = product(oc, 2 * j + b).astype(jnp.bfloat16).reshape(4, ROWS, 256)

        def hold(j):
            for b in (0, 1):
                keep[j, b] = product(c, 2 * j + b).reshape(4, ROWS, 256)

        def chip(j, b, k, rows):
            return keep[j, b, xs[k], rows] + rb[h, j, b, xs[k], rows].astype(jnp.float32)

        every, low, high = slice(0, 128), slice(0, 64), slice(64, 128)

        def far(j):
            for b in (0, 1):
                u1[h, j, 0, b] = chip(j, b, 2, low).astype(jnp.bfloat16)
                u1[h, j, 1, b] = chip(j, b, 2, high).astype(jnp.bfloat16)

        def near(j, d):
            e, some, rest = (0, low, high) if d == 1 else (1, high, low)
            for b in (0, 1):
                both = chip(j, b, d, some) + r1[h, j, e, b].astype(jnp.float32)
                u2[h, j, e, b, some] = both.astype(jnp.bfloat16)
                u2[h, j, e, b, rest] = chip(j, b, d, rest).astype(jnp.bfloat16)

        def last(j):
            for b in (0, 1):
                s, k = origin(2 * j + b)
                cols = pl.ds(pl.multiple_of(zs[-s * k] * 256, 256), 256)
                total = chip(j, b, 0, every)
                total += r2[h, j, 0, b].astype(jnp.float32) + r2[h, j, 1, b].astype(jnp.float32)
                add(cols, total)

        for j in range(4):
            needs = [(n, "act")]
            for i in (2 * j, 2 * j + 1):
                s, k = origin(i)
                s = -1 if k == 4 else s
                needs += [(m, "a2", s, q, k) for q in (0, 1)]
                needs += [(m, "b1", i) if i else (m, "land")]
                needs += [(m, "h2", 1, i), (m, "h2", -1, i), (m, "h2w", i)]
            plan.add(
                (n, "s0", j), 0.5 + 0.1 * j, work=lambda j=j: give(j), time=0.62, after=needs,
                send=[((n, "r0", j), sb.at[h, j], rb.at[h, j], sib, "c")],
            )
            plan.add((n, "s0k", j), 0.5 + 0.1 * j, work=lambda j=j: hold(j), time=0.62, after=[(n, "s0", j)])
            plan.add(
                (n, "s1", j), 0.2, recv=[((n, "r0", j), rb.at[h, j], sib)], after=[(n, "s0k", j)],
                work=lambda j=j: far(j), time=0.05,
                send=[
                    ((n, "r1", d, j), u1.at[h, j, 0 if d == 1 else 1], r1.at[h, j, 0 if d == 1 else 1], xdev[d], f"x{d}")
                    for d in (1, -1)
                ],
            )
            for d in (1, -1):
                e = 0 if d == 1 else 1
                plan.add(
                    (n, "s2", d, j), 0.1, recv=[((n, "r1", d, j), r1.at[h, j, e], xdev[-d])],
                    after=[(n, "s1", j)], work=lambda j=j, d=d: near(j, d), time=0.05,
                    send=[((n, "r2", d, j), u2.at[h, j, e], r2.at[h, j, e], xdev[d], f"x{d}")],
                )
            plan.add(
                (n, "s3", j), 0.3,
                recv=[((n, "r2", d, j), r2.at[h, j, 0 if d == 1 else 1], xdev[-d]) for d in (1, -1)],
                after=[(n, "s1", j)], work=lambda j=j: last(j), time=0.1,
            )

    def to_middle(cols, total):
        mid[:, cols] = (xown[:, cols].astype(jnp.float32) + 0.5 * total).astype(jnp.bfloat16)

    def to_result(cols, total):
        out_ref[:, cols] = (mid[:, cols].astype(jnp.float32) + 0.5 * total).astype(jnp.bfloat16)

    gather(1, xown, gain1, xn1, [(1, "b1s"), (1, "a1s"), (1, "h1", 0)])
    hidden(1, 1, xn1, ga1, gb1, [])
    scatter(1, 2, da1, db1, to_middle)
    gather(2, mid, gain2, xn2, [(1, "s3", j) for j in range(4)])
    hidden(2, 3, xn2, ga2, gb2, [(1, "act")])
    scatter(2, 4, da2, db2, to_result)

    for name in plan.order():
        rank, recv, work, time, send, after = plan.tasks[name]
        with jax.named_scope("_".join(str(p) for p in name)):
            for key, ref, device in recv:
                net.recv(key, ref, device)
            if work is not None:
                work()
            for key, src, dst, device, link in send:
                net.send(key, src, dst, device)
    net.finish()


def layer(*args):
    bf, f32 = jnp.bfloat16, jnp.float32
    hbm = pl.BlockSpec(memory_space=pl.ANY)
    vmem = pl.BlockSpec(memory_space=pltpu.VMEM)
    pair = (2, 4, 2)
    return pl.pallas_call(
        kernel,
        out_shape=jax.ShapeDtypeStruct((ROWS, D), bf),
        in_specs=[hbm] * 8 + [vmem] * 2,
        out_specs=vmem,
        scratch_shapes=[
            pltpu.VMEM((ROWS, D), bf),
            pltpu.VMEM((ROWS, D), bf),
            pltpu.VMEM((NY, NZ, 64, GA), bf),
            pltpu.VMEM((NY, NZ, 64, GB), bf),
            pltpu.VMEM((NY, NZ, 64, GA), bf),
            pltpu.VMEM((NY, NZ, 64, GB), bf),
            pltpu.VMEM((NZ, NY, 64, DA), bf),
            pltpu.VMEM((NZ, NY, 64, DB), bf),
            pltpu.VMEM((NZ, NY, 64, DA), bf),
            pltpu.VMEM((NZ, NY, 64, DB), bf),
            pltpu.VMEM((4, 2, NX, ROWS, CH), bf),
            pltpu.VMEM((4, 2, NX, ROWS, CH), bf),
            pltpu.VMEM((2, 4 * ROWS, GA), f32),
            pltpu.VMEM((2, 4 * ROWS, GB), f32),
            pltpu.VMEM((2, 4 * ROWS, DK), bf),
            pltpu.VMEM((4, 2, NX, ROWS, 256), f32),
            pltpu.VMEM((*pair, NX, ROWS, 256), bf),
            pltpu.VMEM((*pair, NX, ROWS, 256), bf),
            pltpu.VMEM((*pair, 2, ROWS // 2, 256), bf),
            pltpu.VMEM((*pair, 2, ROWS, 256), bf),
            pltpu.VMEM((*pair, 2, ROWS // 2, 256), bf),
            pltpu.VMEM((*pair, 2, ROWS, 256), bf),
            pltpu.SemaphoreType.DMA((11,)),
            pltpu.SemaphoreType.DMA((SEMS,)),
            pltpu.SemaphoreType.DMA((SEMS,)),
        ],
        compiler_params=pltpu.CompilerParams(
            collective_id=0, has_side_effects=True, vmem_limit_bytes=60 * 2**20
        ),
    )(*args)


def on_device(tokens, norm_one, gate_one, up_one, down_one, norm_two, gate_two, up_two, down_two):
    def rest(gate, up, turned):
        return [gate[:, 512:], up[:, 512:], turned[:, DA:], jnp.zeros((64, DK - H), turned.dtype)]

    turned_one, turned_two = down_one.T, down_two.T
    parts = jnp.concatenate(rest(gate_one, up_one, turned_one) + rest(gate_two, up_two, turned_two), axis=1)
    return layer(
        tokens, gate_one, up_one, turned_one, gate_two, up_two, turned_two, parts,
        norm_one.reshape(1, D), norm_two.reshape(1, D),
    )


def solution(mesh):
    return jax.shard_map(
        on_device,
        mesh=mesh,
        in_specs=(
            P(("fs", "tp"), None),
            P(),
            P("fs", "tp"),
            P("fs", "tp"),
            P("tp", "fs"),
            P(),
            P("fs", "tp"),
            P("fs", "tp"),
            P("tp", "fs"),
        ),
        out_specs=P(("fs", "tp"), None),
        check_vma=False,
    )
```

time: 406 us -> 151 us (0.37)
  waiting for transfers between devices: 303 us -> 0 us
  Pallas kernels: 0 us -> 146 us
  matrix products: 40.4 us -> 0 us
  starting transfers between devices: 27 us -> 0 us
  other arithmetic: 16.4 us -> 0 us
  between operations: 13.2 us -> 0.05 us
    all_gather x3 -> x0, waiting for transfers between devices: 185 us -> none  [the longest x2 161 us: in_one_piece(): result = lax.all_gather(both, axis, axis=dim, tiled=True)]
    pallas_call x0 -> x1, Pallas kernels: none -> 146 us  [layer(): pl.pallas_call(kernel, out_shape=jax.ShapeDtypeStruct((ROWS, D), bf), in_...]
    psum x1 -> x0, waiting for transfers between devices: 68.2 us -> none  [on_device(): lax.psum(first_terms.astype(jnp.bfloat16), 'tp').astype(jnp.float32)]
    all_to_all x3 -> x0, waiting for transfers between devices: 48.8 us -> none  [the longest x1 48.8 us: summed_on_arrival(): lax.all_to_all(parts, axis, split_axis=0, concat_axis=0, tiled=True)]
    dot_general x4 -> x0, matrix products: 40.4 us -> none  [the longest x2 26 us: down_terms(): jnp.dot(hidden, gathered_copies(down_w, 'fs', 1), preferred_element_type=...]
    all_to_all x3 -> x0, starting transfers between devices: 26.9 us -> none  [the longest x2 18.1 us: copy_for_each(): return lax.all_to_all(copies, axis, split_axis=0, concat_axis=0, tiled=True)]
    reduce_sum x3 -> x0, other arithmetic: 12 us -> none  [the longest x2 9.03 us: normalize(): jnp.mean(values * values, axis=-1, keepdims=True) + eps]
    broadcast_in_dim x2 -> x0, local copies, waits for them, and re-layouts: 4.55 us -> none  [copy_for_each(): copies = jnp.broadcast_to(shard, (lax.axis_size(axis), *shard.shape))]
  transfers between devices with their start and end apart: 7 -> 0, of which waited for: 5 -> 0; matrix products, arithmetic and copies ran while one was open for 8% -> 0% of each run, Pallas kernels for 0% -> 0%
where the time goes in v2:
time: 151 us; the launch traced here: 150 us
  Pallas kernels  146 us (97%)
  local copies, waits for them, and re-layouts  4.32 us (3%)
    pallas_call x1, Pallas kernels, layer(): pl.pallas_call(kernel, out_shape=jax.ShapeDtypeStruct((ROWS, D), bf), in_...  146 us

profile of v2, /device:TPU:1, one launch (start us, length us, event | category | flops | bytes accessed | tf_op | source)
XLA Modules:
  0.0 150.3 jit_solution(9122315374374392126)
XLA Ops:
  0.0 0.0 copy-start
  0.0 0.0 copy-start.1
  0.0 0.9 copy-done
  0.9 0.0 copy-done.1
  0.9 0.0 slice-start.1
  0.9 0.0 slice-start.2
  0.9 0.0 slice-start.3
  1.0 0.0 slice-start
  1.0 0.7 slice-done.1
  1.6 0.0 slice-done.2
  1.7 0.0 slice-done.3
  1.7 0.0 slice-done
  1.7 0.8 concatenate.3.rest_in
  2.5 145.9 %shard_map.91 = bf16[128,2048]{1,0:T(8,128)(2,1)} custom-call(bf16[128,2048]{1,0:T(8,128)(2,1)} %x_in.1, bf16[64,576]{1,0:T(8,128)(2,1)} %gate1_in.1, bf16[64,576]{1,0:T(8,128)(2,1)} %up1_in.1, bf16[64,576]{1,0:T(8,128)(2,1)} %bitcast.4, bf16[64,576]{1,0:T(8,128)(2,1)} %gate2_in.1, bf16[64,576]{1,0:T(8,128)(2,1)} %up2_in.1, bf16[64,576]{1,0:T(8,128)(2,1)} %bitcast.6, ...), custom_call_target="tpu_custom_call" | custom-call | tf_op jit(solution)/shard_map/pallas_call | solution.py:447
  148.4 1.9 %copy.11 = bf16[128,2048]{1,0:T(8,128)(2,1)} copy(bf16[128,2048]{1,0:T(8,128)(2,1)} %shard_map.91) | data formatting | bytes 1048576
  (3 shorter events, 0.0 us)
Async XLA Ops:
  0.0 0.9 copy-start
  0.0 0.9 copy-start.1
  0.9 0.7 slice-start.1
  0.9 0.7 slice-start.2
  0.9 0.7 slice-start.3
  1.0 0.8 slice-start
